TPU v7x, 32 devices: a whole 2x2x4 slice. The times are simulated.
32 devices in a mesh: sp: 8 (over z, x), tp: 4 (over y, core).
Axes of the slice: x: 2, y: 2, z: 4, core: 2. Of those that a mesh axis runs over, the one named last changes fastest.
Arguments:
- queries: bfloat16 [2048, 1536], P('sp', 'tp'), may hold values from -500 to 500
- latent: bfloat16 [2048, 256], P('sp'), may hold values from -6 to 6
- rope_key: bfloat16 [2048, 32], P('sp'), may hold values from -6 to 6
- latent_gain: bfloat16 [256], replicated, may hold values from 0.099609375 to 1.8984375
- key_value_weight: bfloat16 [256, 2048], P(None, 'tp'), may hold values from -0.375 to 0.375
- out_weight: bfloat16 [1024, 2048], P(None, 'tp'), may hold values from -6 to 6
- residual: bfloat16 [2048, 2048], P('sp', 'tp'), may hold values from -150 to 150
- ffn_gain: bfloat16 [2048], replicated, may hold values from 0.099609375 to 1.8984375
- routes: int32 [2048, 2], P('sp'), may hold values from 0 to 7, all different within a row; in each aligned block of 256 rows (0 to 255, 256 to 511, ...) at most 128 rows name the same one
- route_prob: float32 [2048, 2], P('sp'), may hold values from 0.1 to 1
- group_weight: float32 [2048], P('sp'), may hold values from 0.25 to 1
- gate_weight: bfloat16 [8, 2048, 4096], P('sp', None, 'tp'), may hold values from -0.125 to 0.125
- up_weight: bfloat16 [8, 2048, 4096], P('sp', None, 'tp'), may hold values from -0.125 to 0.125
- down_weight: bfloat16 [8, 4096, 2048], P('sp', None, 'tp'), may hold values from -0.75 to 0.75
Outputs:
- final: bfloat16 [2048, 2048], P('sp', 'tp')
Inputs may be any that keep to these rules, and one draw needn't show every extreme that they name: `routes`: each row names 2 different experts; among the 256 rows of one index of sp no expert is named more than 128 times, a bound that some block reaches.
All inputs are finite; a program needn't handle non-finite values.
Results may differ from a plain program's by a relative error of at most 0.015.
The roundings to bfloat16 on the way count: a program that leaves them out, or rounds other values in their place, can miss the bound.
Values may be sent and summed in bfloat16 or wider, within the bound.
A program may use at most 64 MiB of HBM per device.

v0:
```python
import jax
import jax.numpy as jnp
from jax import lax
from jax.sharding import PartitionSpec as P

D = 2048
NOPE = 64
ROPE = 32
VDIM = 64
TOP = 2
SPAN = 64
EXP_DEV = 1


THETA = 500000.0
EPSILON = 1e-06


def rotate(values, positions):
    rot_width = values.shape[-1]
    half_width = rot_width // 2
    frequency = 1.0 / THETA ** (jnp.arange(0, rot_width, 2, dtype=jnp.float32) / rot_width)
    angles = positions.astype(jnp.float32)[:, None] * frequency[None, :]
    view_shape = (values.shape[0],) + (1,) * (values.ndim - 2) + (half_width,)
    cos_table = jnp.cos(angles).reshape(view_shape)
    sin_table = jnp.sin(angles).reshape(view_shape)
    wide = values.astype(jnp.float32)
    lower_half = wide[..., :half_width]
    upper_half = wide[..., half_width:]
    return jnp.concatenate(
        [
            lower_half * cos_table - upper_half * sin_table,
            upper_half * cos_table + lower_half * sin_table,
        ],
        axis=-1,
    )


def body(
    queries,
    latent,
    rope_key,
    latent_gain,
    key_value_weight,
    out_weight,
    residual,
    ffn_gain,
    routes,
    route_prob,
    group_weight,
    gate_weight,
    up_weight,
    down_weight,
):
    tokens_here = queries.shape[0]
    heads_here = key_value_weight.shape[1] // (NOPE + VDIM)
    width_here = residual.shape[1]
    offset = lax.axis_index("sp") * tokens_here
    positions = offset + jnp.arange(tokens_here, dtype=jnp.int32)
    query = queries.reshape(tokens_here, heads_here, NOPE + ROPE)
    query_nope = query[..., :NOPE]
    query_rope = rotate(query[..., NOPE:], positions).astype(jnp.bfloat16)
    query_blocks = positions // SPAN
    last_block = query_blocks[-1]
    scaling = (NOPE + ROPE) ** (-0.5)

    def project(latent_rows, rope_rows):
        length = latent_rows.shape[0]
        latent_wide = latent_rows.astype(jnp.float32)
        normed = latent_wide * lax.rsqrt(
            jnp.mean(latent_wide * latent_wide, axis=-1, keepdims=True) + EPSILON
        )
        normed = (normed * latent_gain.astype(jnp.float32)).astype(jnp.bfloat16)
        key_value = jnp.dot(normed, key_value_weight, preferred_element_type=jnp.float32).astype(
            jnp.bfloat16
        )
        rotated = rotate(rope_rows, jnp.arange(length, dtype=jnp.int32)).astype(jnp.bfloat16)
        return (key_value, rotated)

    def attend(state_in, key_value, rotated):
        length = rotated.shape[0]
        running_max, normalizer, weighted = state_in
        key_value = key_value.reshape(length, heads_here, NOPE + VDIM)
        scores = jnp.einsum(
            "qhd,khd->qhk", query_nope, key_value[..., :NOPE], preferred_element_type=jnp.float32
        )
        scores = scores + jnp.einsum(
            "qhd,kd->qhk", query_rope, rotated, preferred_element_type=jnp.float32
        )
        scores = scores * scaling
        key_blocks = jnp.arange(length, dtype=jnp.int32) // SPAN
        allowed = key_blocks[None, :] <= query_blocks[:, None]
        scores = jnp.where(allowed[:, None, :], scores, -jnp.inf)
        new_max = jnp.maximum(running_max, jnp.max(scores, axis=-1))
        exp_scores = jnp.exp(scores - new_max[..., None])
        normalizer = jnp.sum(exp_scores, axis=-1)
        weighted = jnp.einsum(
            "qhk,khd->qhd",
            exp_scores.astype(jnp.bfloat16),
            key_value[..., NOPE:],
            preferred_element_type=jnp.float32,
        )
        return (new_max, normalizer, weighted)

    initial = (
        jnp.full((tokens_here, heads_here), -1e30, jnp.float32),
        jnp.zeros((tokens_here, heads_here), jnp.float32),
        jnp.zeros((tokens_here, heads_here, VDIM), jnp.float32),
    )
    pieces = (
        lax.all_gather(latent, "sp", axis=0, tiled=True),
        lax.all_gather(rope_key, "sp", axis=0, tiled=True),
    )

    def attend_piece(kept):
        key_value, rotated = project(pieces[0], pieces[1])
        return attend(kept, key_value, rotated)

    running_max, normalizer, weighted = lax.cond(
        jnp.int32(0) // SPAN > last_block, lambda kept: kept, attend_piece, initial
    )
    attended = (
        (weighted / normalizer[..., None])
        .astype(jnp.bfloat16)
        .reshape(tokens_here, heads_here * VDIM)
    )
    projected = jnp.dot(
        lax.all_gather(attended, "tp", axis=1, tiled=True),
        out_weight,
        preferred_element_type=jnp.float32,
    )
    mixed_rows = (residual.astype(jnp.float32) + projected).astype(jnp.bfloat16)
    mixed_wide = mixed_rows.astype(jnp.float32)
    sp_count = lax.axis_size("sp")
    experts_all = EXP_DEV * sp_count
    capacity = 2 * tokens_here * TOP // experts_all
    picks = routes.reshape(-1)
    onehot = (picks[:, None] == jnp.arange(experts_all, dtype=jnp.int32)[None, :]).astype(jnp.int32)
    slot_index = jnp.sum((jnp.cumsum(onehot, axis=0) - 1) * onehot, axis=1)
    target = picks * capacity + slot_index
    token_of = jnp.arange(tokens_here * TOP, dtype=jnp.int32) // TOP
    row_shape = (sp_count, EXP_DEV, capacity)

    def place(source_rows):
        empty = jnp.zeros((experts_all * capacity,) + source_rows.shape[1:], source_rows.dtype)
        filled = empty.at[target].set(source_rows[token_of])
        return filled.reshape((sp_count, EXP_DEV * capacity) + source_rows.shape[1:])

    row_squares = lax.psum(jnp.sum(mixed_wide * mixed_wide, axis=-1), "tp")
    row_scale = lax.rsqrt(row_squares / D + EPSILON)
    gain_here = lax.dynamic_slice_in_dim(
        ffn_gain, lax.axis_index("tp") * width_here, width_here, 0
    ).astype(jnp.float32)
    scaled = (mixed_wide * gain_here[None, :]).astype(jnp.bfloat16)
    arrived_rows, arrived_scale = (
        lax.all_to_all(place(scaled), "sp", split_axis=0, concat_axis=0, tiled=True),
        lax.all_to_all(
            place(row_scale).astype(jnp.bfloat16), "sp", split_axis=0, concat_axis=0, tiled=True
        ).astype(jnp.float32),
    )
    part_rows = lax.all_gather(arrived_rows, "tp", axis=2, tiled=True)
    inputs = part_rows.reshape(row_shape + (part_rows.shape[2],))
    length = inputs.shape[3]
    gate_acc = jnp.einsum("secd,edf->secf", inputs, gate_weight, preferred_element_type=jnp.float32)
    up_acc = jnp.einsum("secd,edf->secf", inputs, up_weight, preferred_element_type=jnp.float32)
    row_scales = arrived_scale.reshape(row_shape)
    gate_full = gate_acc * row_scales[..., None]
    up_full = up_acc * row_scales[..., None]
    hidden = (jax.nn.silu(gate_full) * up_full).astype(jnp.bfloat16)
    expert_out = jnp.einsum(
        "secf,efd->secd",
        lax.all_gather(hidden, "tp", axis=3, tiled=True),
        down_weight,
        preferred_element_type=jnp.float32,
    ).astype(jnp.bfloat16)
    returned_rows = lax.all_to_all(
        expert_out.reshape(sp_count, EXP_DEV * capacity, width_here),
        "sp",
        split_axis=0,
        concat_axis=0,
        tiled=True,
    )
    picked = (
        returned_rows.reshape(experts_all * capacity, width_here)[target]
        .astype(jnp.float32)
        .reshape(tokens_here, TOP, width_here)
    )
    combine = group_weight[:, None] * route_prob / jnp.sum(route_prob, axis=-1, keepdims=True)
    routed_sum = jnp.sum(combine[..., None] * picked, axis=1)
    return (mixed_wide + routed_sum).astype(jnp.bfloat16)


def solution(mesh):
    return jax.shard_map(
        body,
        mesh=mesh,
        in_specs=(
            P("sp", "tp"),
            P("sp", None),
            P("sp", None),
            P(),
            P(None, "tp"),
            P(None, "tp"),
            P("sp", "tp"),
            P(),
            P("sp", None),
            P("sp", None),
            P("sp"),
            P("sp", None, "tp"),
            P("sp", None, "tp"),
            P("sp", None, "tp"),
        ),
        out_specs=P("sp", "tp"),
        check_vma=False,
    )
```

profile of v0, /device:TPU:0, one launch (start us, length us, event | category | flops | bytes accessed | tf_op | source)
XLA Modules:
  0.0 265.6 jit_solution(10837312573786537266)
XLA Ops:
  6.5 0.7 all-gather.4.cloned.1.call-update
  7.3 0.8 copy.38
  8.4 0.7 broadcast_multiply_fusion
  9.1 1.1 copy.35
  11.4 1.1 reduce-window.6
  13.1 32.9 %all_gather.16 = bf16[2048,32]{0,1:T(8,128)(2,1)S(1)} all-gather(bf16[256,32]{0,1:T(8,128)(2,1)} %param.18), channel_id=1, replica_groups=mesh['sp'=8,'tp'=4] {'sp'}, dimensions={0}, use_global_device_ids=true | all-gather | bytes 147456 | tf_op jit(solution)/shard_map/all_gather | solution.py:112
  46.0 0.8 dynamic-slice_convert_fusion
  47.1 5.7 %all-gather.4.cloned.1.call-done = bf16[2048,256]{1,0:T(8,128)(2,1)} async-done(((bf16[256,256]{1,0:T(8,128)(2,1)}), bf16[2048,256]{1,0:T(8,128)(2,1)}) %all-gather.4.cloned.1.call-update) | async-done | bytes 1048592 | tf_op jit(solution)/shard_map/all_gather | solution.py:111
  52.8 11.5 %conditional.1 = (f32[256,4]{0,1:T(4,128)S(1)}, f32[256,4,64]{0,2,1:T(8,128)S(1)}) conditional(s32[]{:T(128)} %bitcast.5, (s32[256]{0:T(256)S(1)}, bf16[2048,256]{1,0:T(8,128)(2,1)}, bf16[256]{0:T(256)(128)(2,1)}, bf16[256,512]{1,0:T(8,128)(2,1)}, bf16[256,4,96]{0,2,1:T(8,128)(2,1)S(1)}, /*index=5*/bf16[2048,32]{0,1:T(8,128)(2,1)S(1)}, ...), branch_computations={%region_0.4_spmd, %region_4.5_spmd} | conditional | flops 1230621952 | bytes 51015312 | solution.py:119
  52.8 1.6 fusion.7
  55.1 2.1 convolution_convert_fusion
  57.2 1.3 fusion.15
  59.6 2.1 fusion.62
  61.8 1.4 fusion.10
  63.2 1.1 fusion.3
  64.4 7.3 %all_gather.17 = bf16[256,1024]{0,1:T(8,128)(2,1)S(1)} all-gather(bf16[256,256]{0,1:T(8,128)(2,1)S(1)} %bitcast.94), channel_id=1, replica_groups=mesh['sp'=8,'tp'=4] {'tp'}, dimensions={1}, use_global_device_ids=true | all-gather | bytes 655360 | tf_op jit(solution)/shard_map/all_gather | solution.py:128
  72.2 5.1 %scatter_custom_fusion = bf16[1024,512]{1,0:T(8,128)(2,1)S(1)} fusion(s32[512]{0:T(512)S(1)} %bitcast.95, bf16[256,512]{1,0:T(8,128)(2,1)S(1)} %get-tuple-element.40, s32[1024]{0:T(1024)S(1)} %pad_clamp_fusion.1, bf16[]{:T(256)} %constant.125.clone.1), kind=kCustom, calls=%fused_computation.70 | custom fusion | bytes 1048578 | tf_op jit(solution)/shard_map/scatter | solution.py:146
  77.3 29.6 %all_to_all.16 = bf16[8,128,512]{2,1,0:T(8,128)(2,1)} all-to-all(bf16[8,128,512]{2,1,0:T(8,128)(2,1)S(1)} %bitcast.91), channel_id=1, replica_groups=mesh['sp'=8,'tp'=4] {'sp'}, dimensions={0} | all-to-all | bytes 2097152 | tf_op jit(solution)/shard_map/all_to_all | solution.py:156
  107.0 5.7 %psum.7 = f32[256]{0:T(256)S(1)} all-reduce(f32[256]{0:T(256)S(1)} %get-tuple-element.39), channel_id=1, replica_groups=mesh['sp'=8,'tp'=4] {'tp'}, use_global_device_ids=true, to_apply=%region_11.12 | all-reduce | flops 256 | bytes 2048 | tf_op jit(solution)/shard_map/psum | solution.py:149
  112.6 3.5 %gather_fusion = f32[512]{0:T(512)S(1)} fusion(f32[256]{0:T(256)S(1)} %add_rsqrt_fusion.1, s32[1024]{0:T(1024)S(1)} %pad_clamp_fusion.1), kind=kCustom, calls=%fused_computation.1 | custom fusion | bytes 6144 | tf_op jit(solution)/shard_map/gather | solution.py:146
  116.2 2.4 scatter_custom_fusion.1
  118.6 10.5 %all_to_all.17 = bf16[8,1,128]{2,1,0:T(2,128)(2,1)S(1)} all-to-all(bf16[8,1,128]{2,1,0:T(2,128)(2,1)S(1)} %copy.40), channel_id=1, replica_groups=mesh['sp'=8,'tp'=4] {'sp'}, dimensions={0} | all-to-all | bytes 4096 | tf_op jit(solution)/shard_map/all_to_all | solution.py:157
  129.1 10.8 %all-gather.6.cloned.1.call-done = bf16[8,128,2048]{2,1,0:T(8,128)(2,1)} async-done(((bf16[8,128,512]{2,1,0:T(8,128)(2,1)}), bf16[8,128,2048]{2,1,0:T(8,128)(2,1)}) %all-gather.6.cloned.1.call-update) | async-done | bytes 4194320 | tf_op jit(solution)/shard_map/all_gather | solution.py:161
  139.9 7.6 %fusion.41 = f32[8,128,1024]{2,1,0:T(8,128)S(1)} fusion(bf16[8,128,2048]{2,1,0:T(8,128)(2,1)} %all-gather.6.cloned.1.call-done, bf16[1,2048,1024]{2,1,0:T(8,128)(2,1)} %param.28), kind=kOutput, calls=%fused_computation.61 | convolution fusion | flops 4294967296 | bytes 12582912 | tf_op jit(solution)/shard_map/secd,edf->secf/dot_general | solution.py:165
  147.6 6.4 %fusion.38 = bf16[8,1,128,1024]{3,2,0,1:T(8,128)(2,1)} fusion(f32[8,128,1024]{2,1,0:T(8,128)S(1)} %fusion.41, bf16[8,128,2048]{2,1,0:T(8,128)(2,1)S(1)} %copy-done.4, bf16[1,2048,1024]{2,1,0:T(8,128)(2,1)S(1)} %copy-done.3, f32[8,128]{1,0:T(8,128)S(1)} %bitcast.100), kind=kOutput, calls=%fused_computation.57 | convolution fusion | flops 4303355904 | bytes 14684160 | tf_op jit(solution)/shard_map/secd,edf->secf/dot_general | solution.py:164
  154.1 58.4 %all-gather.8.cloned.1.call-done = bf16[8,1,128,4096]{3,2,0,1:T(8,128)(2,1)} async-done(((bf16[8,1,128,1024]{3,2,0,1:T(8,128)(2,1)}), bf16[8,1,128,4096]{3,2,0,1:T(8,128)(2,1)}) %all-gather.8.cloned.1.call-update) | async-done | bytes 8388624 | tf_op jit(solution)/shard_map/all_gather | solution.py:172
  212.5 10.1 %fusion.47 = bf16[8,128,512]{2,1,0:T(8,128)(2,1)} fusion(bf16[1,4096,512]{2,1,0:T(8,128)(2,1)} %param.29, bf16[8,1,128,4096]{3,2,0,1:T(8,128)(2,1)} %all-gather.8.cloned.1.call-done), kind=kOutput, calls=%fused_computation.65 | convolution fusion | flops 4295491584 | bytes 13631488 | tf_op jit(solution)/shard_map/secf,efd->secd/dot_general | solution.py:170
  222.6 5.5 %all-to-all-start.2 = ((bf16[8,128,512]{2,1,0:T(8,128)(2,1)}), bf16[8,128,512]{2,1,0:T(8,128)(2,1)S(1)}, u32[]{:S(2)}, u32[]{:S(2)}) async-start(bf16[8,128,512]{2,1,0:T(8,128)(2,1)} %fusion.47), calls=%async_computation.2 | async-start | bytes 2097152 | tf_op jit(solution)/shard_map/all_to_all | solution.py:176
  228.3 26.0 %all-to-all-done.2 = bf16[8,128,512]{2,1,0:T(8,128)(2,1)S(1)} async-done(((bf16[8,128,512]{2,1,0:T(8,128)(2,1)}), bf16[8,128,512]{2,1,0:T(8,128)(2,1)S(1)}, u32[]{:S(2)}, u32[]{:S(2)}) %all-to-all-start.2) | async-done | bytes 1048608 | tf_op jit(solution)/shard_map/all_to_all | solution.py:176
  254.3 2.0 gather_fusion.1
  256.9 1.3 multiply_reduce_fusion
  258.2 0.8 add_convert_fusion
  (57 shorter events, 5.0 us)
Async XLA Ops:
  6.5 65.1 %copy-start = (bf16[1024,512]{1,0:T(8,128)(2,1)S(1)}, bf16[1024,512]{1,0:T(8,128)(2,1)}, u32[]{:S(2)}) copy-start(bf16[1024,512]{1,0:T(8,128)(2,1)} %param.21) | copy-start | bytes 3145732
  6.5 46.3 %all-gather.4.cloned.1.call-start = ((), (), s32[]{:S(2)}) async-start(), calls=%async_computation.3 | async-start | bytes 1179648 | tf_op jit(solution)/shard_map/all_gather | solution.py:111
  7.3 132.7 %all-gather.6.cloned.1.call-start = ((), (), s32[]{:S(2)}) async-start(), calls=%async_computation.4 | async-start | bytes 5242880 | tf_op jit(solution)/shard_map/all_gather | solution.py:161
  52.8 18.9 %copy-start.5 = (bf16[256,512]{1,0:T(8,128)(2,1)S(1)}, bf16[256,512]{1,0:T(8,128)(2,1)}, u32[]{:S(2)}) copy-start(bf16[256,512]{1,0:T(8,128)(2,1)} %param.22) | copy-start | bytes 786436
  106.9 105.5 %all-gather.8.cloned.1.call-start = ((), (), s32[]{:S(2)}) async-start(), calls=%async_computation.5 | async-start | bytes 10485760 | tf_op jit(solution)/shard_map/all_gather | solution.py:172
  139.9 7.7 %copy-start.3 = (bf16[1,2048,1024]{2,1,0:T(8,128)(2,1)S(1)}, bf16[1,2048,1024]{2,1,0:T(8,128)(2,1)}, u32[]{:S(2)}) copy-start(bf16[1,2048,1024]{2,1,0:T(8,128)(2,1)} %param.27) | copy-start | bytes 12582916
  139.9 7.7 %copy-start.4 = (bf16[8,128,2048]{2,1,0:T(8,128)(2,1)S(1)}, bf16[8,128,2048]{2,1,0:T(8,128)(2,1)}, u32[]{:S(2)}) copy-start(bf16[8,128,2048]{2,1,0:T(8,128)(2,1)} %all-gather.6.cloned.1.call-done) | copy-start | bytes 12582916
  154.0 74.1 %copy-start.1 = (f32[256,2]{0,1:T(2,128)S(1)}, f32[256,2]{0,1:T(2,128)}, u32[]{:S(2)}) copy-start(f32[256,2]{0,1:T(2,128)} %param.25) | copy-start | bytes 6148
  154.0 74.1 %copy-start.2 = (f32[256]{0:T(256)S(1)}, f32[256]{0:T(256)}, u32[]{:S(2)}) copy-start(f32[256]{0:T(256)} %param.26) | copy-start | bytes 3076
  222.6 31.7 %all-to-all-start.2 = ((bf16[8,128,512]{2,1,0:T(8,128)(2,1)}), bf16[8,128,512]{2,1,0:T(8,128)(2,1)S(1)}, u32[]{:S(2)}, u32[]{:S(2)}) async-start(bf16[8,128,512]{2,1,0:T(8,128)(2,1)} %fusion.47), calls=%async_computation.2 | async-start | bytes 2097152 | tf_op jit(solution)/shard_map/all_to_all | solution.py:176
Sparse Core Ops, SparseCore 0:
  9.5 43.2 all-gather.3
  107.0 32.8 all-gather.5
  154.2 58.2 all-gather.7
where the time goes:
time: 266 us
  waiting for transfers between devices  102 us (38%)
  blocking collectives  85.9 us (32%)
  matrix products  31.8 us (12%)
  local copies, waits for them, and re-layouts  17 us (6%)
  between operations  14 us (5%)
  other arithmetic  9.59 us (4%)
  starting transfers between devices  5.59 us (2%)
    all_gather x1, waiting for transfers between devices, body(): lax.all_gather(hidden, 'tp', axis=3, tiled=True)  58.4 us
    all_gather x1, blocking collectives, body(): lax.all_gather(rope_key, 'sp', axis=0, tiled=True)  32.9 us
    all_to_all x1, blocking collectives, body(): lax.all_to_all(place(scaled), 'sp', split_axis=0, concat_axis=0, tiled=True)  29.6 us
    all_to_all x1, waiting for transfers between devices, body(): lax.all_to_all(expert_out.reshape(sp_count, EXP_DEV * capacity, width_her...  26 us
    all_gather x1, waiting for transfers between devices, body(): part_rows = lax.all_gather(arrived_rows, 'tp', axis=2, tiled=True)  10.8 us
    all_to_all x1, blocking collectives, body(): lax.all_to_all(place(row_scale).astype(jnp.bfloat16), 'sp', split_axis=0,...  10.5 us
    dot_general x1, matrix products, body(): jnp.einsum('secf,efd->secd', lax.all_gather(hidden, 'tp', axis=3, tiled=T...  10.1 us
    dot_general x1, matrix products, body(): jnp.einsum('secd,edf->secf', inputs, up_weight, preferred_element_type=jn...  7.64 us
  transfers between devices with their start and end apart: 4, of which 4 were waited for; matrix products, arithmetic and copies ran while one was open for 5% of the time, Pallas kernels for 0%

commit v1 on v0

v1 whole, which is shorter than its diff:
```python
import functools
import jax
import jax.numpy as jnp
from jax import lax
from jax.experimental import pallas as pl
from jax.experimental.pallas import tpu as pltpu
from jax.sharding import PartitionSpec as P

NOPE = 64
ROPE = 32
VDIM = 64
TOP = 2
SPAN = 64
GROUPS = 4
LANES = 128


THETA = 500000.0
EPSILON = 1e-06
MESH = pl.DeviceIdType.MESH


def rotate(values, positions):
    rot_width = values.shape[-1]
    half_width = rot_width // 2
    frequency = 1.0 / THETA ** (jnp.arange(0, rot_width, 2, dtype=jnp.float32) / rot_width)
    angles = positions.astype(jnp.float32)[:, None] * frequency[None, :]
    view_shape = (values.shape[0],) + (1,) * (values.ndim - 2) + (half_width,)
    cos_table = jnp.cos(angles).reshape(view_shape)
    sin_table = jnp.sin(angles).reshape(view_shape)
    wide = values.astype(jnp.float32)
    lower_half = wide[..., :half_width]
    upper_half = wide[..., half_width:]
    return jnp.concatenate(
        [
            lower_half * cos_table - upper_half * sin_table,
            upper_half * cos_table + lower_half * sin_table,
        ],
        axis=-1,
    )


class Links:
    def __init__(self, n_sp, n_tp, send_sem, recv_sem):
        self.n_sp, self.ny = n_sp, n_tp // 2
        self.sp, self.tp = lax.axis_index("sp"), lax.axis_index("tp")
        self.y, self.core = self.tp // 2, self.tp % 2
        self.send_sem, self.recv_sem = send_sem, recv_sem
        self.copies = []

    def barrier(self, over_sp):
        barrier = pltpu.get_barrier_semaphore()
        peers = [(self.sp, self.row(j)) for j in range(1, self.ny)] + [(self.sp, self.twin())]
        if over_sp:
            peers += [((self.sp + r) % self.n_sp, self.tp) for r in range(1, self.n_sp)]
        for peer in peers:
            pl.semaphore_signal(barrier, inc=1, device_id=peer, device_id_type=MESH)
        pl.semaphore_wait(barrier, len(peers))

    def row(self, j):
        return ((self.y + j) % self.ny) * 2 + self.core

    def twin(self):
        return self.y * 2 + (1 - self.core)

    def send(self, src, dst, sp, tp):
        k = len(self.copies)
        copy = pltpu.make_async_remote_copy(
            src_ref=src,
            dst_ref=dst,
            send_sem=self.send_sem.at[k],
            recv_sem=self.recv_sem.at[k],
            device_id=(sp, tp),
            device_id_type=MESH,
        )
        copy.start()
        self.copies.append(copy)
        return copy

    def close(self):
        for copy in self.copies:
            copy.wait_send()


class Spread:
    def __init__(self, links, bufs, g):
        self.links, self.bufs, self.g = links, bufs, g

    def start(self):
        ln = self.links
        self.rows, self.twins = [], []
        for buf in self.bufs:
            mine = buf.at[self.g, ln.tp]
            self.rows.append([ln.send(mine, mine, ln.sp, ln.row(j)) for j in range(1, ln.ny)])
            self.twins.append(ln.send(mine, mine, ln.sp, ln.twin()))

    def relay(self):
        ln = self.links
        for buf, rows in zip(self.bufs, self.rows):
            for j, copy in enumerate(rows, 1):
                copy.wait_recv()
                piece = buf.at[self.g, ln.row(ln.ny - j)]
                self.twins.append(ln.send(piece, piece, ln.sp, ln.twin()))

    def finish(self):
        for copy in self.twins:
            copy.wait_recv()


def copies_of(n_sp, n_tp, groups, exchanged, spreads):
    return exchanged * (n_sp - 1) + spreads * groups * (n_tp - 1)


def latent_kernel(n_sp, n_tp, block_ref, buf, send_sem, recv_sem, local_sem):
    rows = block_ref.shape[0]
    per = n_sp // GROUPS
    links = Links(n_sp, n_tp, send_sem, recv_sem)
    links.barrier(True)
    own = pltpu.make_async_copy(block_ref, buf.at[0, links.tp, pl.ds(0, rows)], local_sem)
    own.start()
    arriving = [own]
    for r in range(1, n_sp):
        g, i = divmod(r, per)
        dst = buf.at[g, links.tp, pl.ds(i * rows, rows)]
        arriving.append(links.send(block_ref, dst, (links.sp + n_sp - r) % n_sp, links.tp))
    spreads = [Spread(links, (buf,), g) for g in range(GROUPS)]
    for g in range(GROUPS):
        for i in range(per):
            r = g * per + i
            if r == 0:
                own.wait()
            else:
                arriving[r].wait_recv()
        spreads[g].start()
        if g > 0:
            spreads[g - 1].relay()
    spreads[-1].relay()
    for spread in spreads:
        spread.finish()
    links.close()


def gather_latents(block, n_sp, n_tp):
    rows, width = block.shape
    count = copies_of(n_sp, n_tp, GROUPS, 1, 1)
    return pl.pallas_call(
        functools.partial(latent_kernel, n_sp, n_tp),
        out_shape=jax.ShapeDtypeStruct((GROUPS, n_tp, n_sp // GROUPS * rows, width), block.dtype),
        in_specs=[pl.BlockSpec(memory_space=pltpu.VMEM)],
        out_specs=pl.BlockSpec(memory_space=pltpu.VMEM),
        scratch_shapes=[
            pltpu.SemaphoreType.DMA((count,)),
            pltpu.SemaphoreType.DMA((count,)),
            pltpu.SemaphoreType.DMA,
        ],
        compiler_params=pltpu.CompilerParams(collective_id=0, has_side_effects=True),
        name="gather_latents",
    )(block)


def attended_kernel(n_sp, n_tp, att_ref, weight_ref, resid_ref, mixed_ref, buf, send_sem, recv_sem, local_sem):
    links = Links(n_sp, n_tp, send_sem, recv_sem)
    depth = att_ref.shape[1]
    links.barrier(False)
    own = pltpu.make_async_copy(att_ref, buf.at[0, links.tp], local_sem)
    own.start()
    own.wait()
    spread = Spread(links, (buf,), 0)
    spread.start()
    spread.relay()
    spread.finish()
    total = jnp.zeros(mixed_ref.shape, jnp.float32)
    for t in range(n_tp):
        total = total + jnp.dot(
            buf[0, t], weight_ref[t * depth : (t + 1) * depth, :], preferred_element_type=jnp.float32
        )
    mixed_ref[...] = (resid_ref[...].astype(jnp.float32) + total).astype(jnp.bfloat16)
    links.close()


def project_attended(attended, weight, residual, n_sp, n_tp):
    count = copies_of(n_sp, n_tp, 1, 0, 1)
    return pl.pallas_call(
        functools.partial(attended_kernel, n_sp, n_tp),
        out_shape=jax.ShapeDtypeStruct(residual.shape, residual.dtype),
        in_specs=[pl.BlockSpec(memory_space=pltpu.VMEM)] * 3,
        out_specs=pl.BlockSpec(memory_space=pltpu.VMEM),
        scratch_shapes=[
            pltpu.VMEM((1, n_tp) + attended.shape, attended.dtype),
            pltpu.SemaphoreType.DMA((count,)),
            pltpu.SemaphoreType.DMA((count,)),
            pltpu.SemaphoreType.DMA,
        ],
        compiler_params=pltpu.CompilerParams(collective_id=1, has_side_effects=True),
        name="project_attended",
    )(attended, weight, residual)


def expert_kernel(
    n_sp, n_tp, placed_ref, squares_ref, gate_hbm, up_hbm, down_hbm, ret_ref,
    rx, sq, hid, ostage, gate_w, up_w, down_w, send_sem, recv_sem, local_sem,
):
    cap, width = placed_ref.shape[1:]
    per = n_sp // GROUPS
    d_model = width * n_tp
    hidden_here = gate_w.shape[1]
    links = Links(n_sp, n_tp, send_sem, recv_sem)
    links.barrier(True)
    own = pltpu.make_async_copy(placed_ref.at[0], rx.at[0, links.tp, pl.ds(0, cap)], local_sem.at[0])
    own_sq = pltpu.make_async_copy(squares_ref.at[0], sq.at[0, links.tp, 0], local_sem.at[1])
    own.start()
    own_sq.start()
    arriving = [None]
    for r in range(1, n_sp):
        g, i = divmod(r, per)
        target = (links.sp + n_sp - r) % n_sp
        arriving.append((
            links.send(squares_ref.at[r], sq.at[g, links.tp, i], target, links.tp),
            links.send(placed_ref.at[r], rx.at[g, links.tp, pl.ds(i * cap, cap)], target, links.tp),
        ))
    loads = [
        pltpu.make_async_copy(gate_hbm.at[0], gate_w, local_sem.at[2]),
        pltpu.make_async_copy(up_hbm.at[0], up_w, local_sem.at[3]),
        pltpu.make_async_copy(down_hbm.at[0], down_w, local_sem.at[4]),
    ]
    for load in loads:
        load.start()
    inputs = [Spread(links, (sq, rx), g) for g in range(GROUPS)]
    hiddens = [Spread(links, (hid,), g) for g in range(GROUPS)]
    returning = []

    def arrive(g):
        for i in range(per):
            r = g * per + i
            if r == 0:
                own.wait()
                own_sq.wait()
            else:
                for copy in arriving[r]:
                    copy.wait_recv()
        inputs[g].start()

    def up_stage(g):
        inputs[g].relay()
        inputs[g].finish()
        if g == 0:
            loads[0].wait()
            loads[1].wait()
        columns = []
        for i in range(per):
            lanes = sq[g, 0, i]
            for t in range(1, n_tp):
                lanes = lanes + sq[g, t, i]
            scale = lax.rsqrt(lanes / d_model + EPSILON)
            columns.append(jnp.broadcast_to(scale[0:1, :], (LANES, LANES)).T[:cap, 0:1])
        scale = jnp.concatenate(columns, axis=0)
        tile = min(256, hidden_here)

        @pl.loop(0, hidden_here // tile)
        def _(n):
            cols = pl.ds(pl.multiple_of(n * tile, tile), tile)
            gate = jnp.zeros((per * cap, tile), jnp.float32)
            upper = jnp.zeros((per * cap, tile), jnp.float32)
            for t in range(n_tp):
                rows = rx[g, t]
                depth = pl.ds(t * width, width)
                gate = gate + jnp.dot(rows, gate_w[depth, cols], preferred_element_type=jnp.float32)
                upper = upper + jnp.dot(rows, up_w[depth, cols], preferred_element_type=jnp.float32)
            gate = gate * scale
            upper = upper * scale
            value = gate / (1.0 + jnp.exp(-gate)) * upper
            hid[g, links.tp, :, cols] = value.astype(jnp.bfloat16)

        hiddens[g].start()

    def down_stage(g):
        hiddens[g].relay()
        hiddens[g].finish()
        if g == 0:
            loads[2].wait()
        tile = min(256, width)

        @pl.loop(0, width // tile)
        def _(n):
            cols = pl.ds(pl.multiple_of(n * tile, tile), tile)
            total = jnp.zeros((per * cap, tile), jnp.float32)
            for t in range(n_tp):
                total = total + jnp.dot(
                    hid[g, t],
                    down_w[pl.ds(t * hidden_here, hidden_here), cols],
                    preferred_element_type=jnp.float32,
                )
            ostage[g, :, cols] = total.astype(jnp.bfloat16)

        for i in range(per):
            r = g * per + i
            piece = ostage.at[g, pl.ds(i * cap, cap)]
            if r == 0:
                back = pltpu.make_async_copy(piece, ret_ref.at[0], local_sem.at[5])
                back.start()
                returning.append(back)
            else:
                returning.append(
                    links.send(piece, ret_ref.at[r], (links.sp + r) % n_sp, links.tp)
                )

    arrive(0)
    arrive(1)
    up_stage(0)
    for g in range(2, GROUPS):
        arrive(g)
        up_stage(g - 1)
    down_stage(0)
    up_stage(GROUPS - 1)
    for g in range(1, GROUPS):
        down_stage(g)
    returning[0].wait()
    for copy in returning[1:]:
        copy.wait_recv()
    links.close()


def run_experts(placed, squares, gate_weight, up_weight, down_weight, n_sp, n_tp):
    cap, width = placed.shape[1:]
    per = n_sp // GROUPS
    hidden_here = gate_weight.shape[2]
    count = copies_of(n_sp, n_tp, GROUPS, 3, 3)
    vmem = pl.BlockSpec(memory_space=pltpu.VMEM)
    hbm = pl.BlockSpec(memory_space=pl.ANY)
    return pl.pallas_call(
        functools.partial(expert_kernel, n_sp, n_tp),
        out_shape=jax.ShapeDtypeStruct(placed.shape, placed.dtype),
        in_specs=[vmem, vmem, hbm, hbm, hbm],
        out_specs=vmem,
        scratch_shapes=[
            pltpu.VMEM((GROUPS, n_tp, per * cap, width), jnp.bfloat16),
            pltpu.VMEM((GROUPS, n_tp, per) + squares.shape[1:], jnp.float32),
            pltpu.VMEM((GROUPS, n_tp, per * cap, hidden_here), jnp.bfloat16),
            pltpu.VMEM((GROUPS, per * cap, width), jnp.bfloat16),
            pltpu.VMEM(gate_weight.shape[1:], jnp.bfloat16),
            pltpu.VMEM(up_weight.shape[1:], jnp.bfloat16),
            pltpu.VMEM(down_weight.shape[1:], jnp.bfloat16),
            pltpu.SemaphoreType.DMA((count,)),
            pltpu.SemaphoreType.DMA((count,)),
            pltpu.SemaphoreType.DMA((6,)),
        ],
        compiler_params=pltpu.CompilerParams(
            collective_id=2, has_side_effects=True, vmem_limit_bytes=50 * 1024 * 1024
        ),
        name="run_experts",
    )(placed, squares, gate_weight, up_weight, down_weight)


def body(
    queries,
    latent,
    rope_key,
    latent_gain,
    key_value_weight,
    out_weight,
    residual,
    ffn_gain,
    routes,
    route_prob,
    group_weight,
    gate_weight,
    up_weight,
    down_weight,
):
    n_sp, n_tp = lax.axis_size("sp"), lax.axis_size("tp")
    sp, tp = lax.axis_index("sp"), lax.axis_index("tp")
    tokens_here, rank = latent.shape
    heads_here = key_value_weight.shape[1] // (NOPE + VDIM)
    width_here = residual.shape[1]
    length = n_sp * tokens_here
    quarter = tokens_here // n_tp

    pad = -(rank + ROPE) % LANES
    block = jnp.concatenate(
        [latent, rope_key, jnp.zeros((tokens_here, pad), latent.dtype)], axis=1
    )
    block = lax.dynamic_slice_in_dim(block, tp * quarter, quarter, 0)
    per = n_sp // GROUPS
    gathered = gather_latents(block, n_sp, n_tp)
    gathered = gathered.reshape(length, rank + ROPE + pad)
    index = jnp.arange(length, dtype=jnp.int32)
    in_quarter = index % quarter
    in_group = index // quarter % per
    of_tp = index // (quarter * per) % n_tp
    group = index // (quarter * per * n_tp)
    source = (sp + group * per + in_group) % n_sp
    key_positions = source * tokens_here + of_tp * quarter + in_quarter

    positions = sp * tokens_here + jnp.arange(tokens_here, dtype=jnp.int32)
    query = queries.reshape(tokens_here, heads_here, NOPE + ROPE)
    query_nope = query[..., :NOPE]
    query_rope = rotate(query[..., NOPE:], positions).astype(jnp.bfloat16)
    scaling = (NOPE + ROPE) ** (-0.5)
    latent_wide = gathered[:, :rank].astype(jnp.float32)
    normed = latent_wide * lax.rsqrt(
        jnp.mean(latent_wide * latent_wide, axis=-1, keepdims=True) + EPSILON
    )
    normed = (normed * latent_gain.astype(jnp.float32)).astype(jnp.bfloat16)
    key_value = jnp.dot(normed, key_value_weight, preferred_element_type=jnp.float32).astype(
        jnp.bfloat16
    )
    rotated = rotate(gathered[:, rank : rank + ROPE], key_positions).astype(jnp.bfloat16)
    key_value = key_value.reshape(length, heads_here, NOPE + VDIM)
    scores = jnp.einsum(
        "qhd,khd->qhk", query_nope, key_value[..., :NOPE], preferred_element_type=jnp.float32
    )
    scores = scores + jnp.einsum(
        "qhd,kd->qhk", query_rope, rotated, preferred_element_type=jnp.float32
    )
    scores = scores * scaling
    allowed = (key_positions // SPAN)[None, :] <= (positions // SPAN)[:, None]
    scores = jnp.where(allowed[:, None, :], scores, -jnp.inf)
    row_max = jnp.max(scores, axis=-1)
    exp_scores = jnp.exp(scores - row_max[..., None])
    normalizer = jnp.sum(exp_scores, axis=-1)
    weighted = jnp.einsum(
        "qhk,khd->qhd",
        exp_scores.astype(jnp.bfloat16),
        key_value[..., NOPE:],
        preferred_element_type=jnp.float32,
    )
    attended = (
        (weighted / normalizer[..., None])
        .astype(jnp.bfloat16)
        .reshape(tokens_here, heads_here * VDIM)
    )
    mixed_rows = project_attended(attended, out_weight, residual, n_sp, n_tp)
    mixed_wide = mixed_rows.astype(jnp.float32)

    capacity = 2 * tokens_here * TOP // n_sp
    picks = routes.reshape(-1)
    onehot = (picks[:, None] == jnp.arange(n_sp, dtype=jnp.int32)[None, :]).astype(jnp.int32)
    slot_index = jnp.sum((jnp.cumsum(onehot, axis=0) - 1) * onehot, axis=1)
    target = ((sp + n_sp - picks) % n_sp * capacity + slot_index).reshape(tokens_here, TOP)
    slots = jnp.arange(n_sp * capacity, dtype=jnp.int32)
    chosen = [target[:, k][None, :] == slots[:, None] for k in range(TOP)]
    anywhere = functools.reduce(jnp.logical_or, chosen)

    part_squares = jnp.sum(mixed_wide * mixed_wide, axis=-1)
    slot_squares = jnp.sum(jnp.where(anywhere, part_squares[None, :], 0.0), axis=1)
    slot_squares = jnp.pad(
        slot_squares.reshape(n_sp, 1, capacity), ((0, 0), (0, 0), (0, LANES - capacity))
    )
    slot_squares = jnp.broadcast_to(slot_squares, (n_sp, 8, LANES))
    gain_here = lax.dynamic_slice_in_dim(ffn_gain, tp * width_here, width_here, 0).astype(
        jnp.float32
    )
    scaled = (mixed_wide * gain_here[None, :]).astype(jnp.bfloat16)
    placed = jnp.dot(
        anywhere.astype(jnp.bfloat16), scaled, preferred_element_type=jnp.float32
    ).astype(jnp.bfloat16)
    returned = run_experts(
        placed.reshape(n_sp, capacity, width_here),
        slot_squares,
        gate_weight,
        up_weight,
        down_weight,
        n_sp,
        n_tp,
    ).reshape(n_sp * capacity, width_here)
    combine = group_weight[:, None] * route_prob / jnp.sum(route_prob, axis=-1, keepdims=True)
    total = mixed_wide
    routed_sum = jnp.zeros_like(mixed_wide)
    for k in range(TOP):
        picked = lax.dot_general(
            chosen[k].astype(jnp.bfloat16),
            returned,
            (((0,), (0,)), ((), ())),
            preferred_element_type=jnp.float32,
        )
        routed_sum = routed_sum + combine[:, k : k + 1] * picked
    return (total + routed_sum).astype(jnp.bfloat16)


def solution(mesh):
    return jax.shard_map(
        body,
        mesh=mesh,
        in_specs=(
            P("sp", "tp"),
            P("sp", None),
            P("sp", None),
            P(),
            P(None, "tp"),
            P(None, "tp"),
            P("sp", "tp"),
            P(),
            P("sp", None),
            P("sp", None),
            P("sp"),
            P("sp", None, "tp"),
            P("sp", None, "tp"),
            P("sp", None, "tp"),
        ),
        out_specs=P("sp", "tp"),
        check_vma=False,
    )
```

time: 266 us -> 157 us (0.59)
  Pallas kernels: 0 us -> 134 us
  waiting for transfers between devices: 102 us -> 0 us
  blocking collectives: 85.9 us -> 0 us
  matrix products: 31.8 us -> 8.4 us
  between operations: 14 us -> 0.3 us
  local copies, waits for them, and re-layouts: 17 us -> 4.84 us
  starting transfers between devices: 5.59 us -> 0 us
    pallas_call x0 -> x3, Pallas kernels: none -> 134 us  [the longest x1 101 us: run_experts(): pl.pallas_call(functools.partial(expert_kernel, n_sp, n_tp), out_shape=ja...]
    all_gather x3 -> x0, waiting for transfers between devices: 74.9 us -> none  [the longest x1 58.4 us: body(): lax.all_gather(hidden, 'tp', axis=3, tiled=True)]
    all_gather x2 -> x0, blocking collectives: 40.1 us -> none  [the longest x1 32.9 us: body(): lax.all_gather(rope_key, 'sp', axis=0, tiled=True)]
    all_to_all x2 -> x0, blocking collectives: 40.1 us -> none  [the longest x1 29.6 us: body(): lax.all_to_all(place(scaled), 'sp', split_axis=0, concat_axis=0, tiled=True)]
    all_to_all x1 -> x0, waiting for transfers between devices: 26 us -> none  [body(): lax.all_to_all(expert_out.reshape(sp_count, EXP_DEV * capacity, width_her...]
    dot_general x8 -> x7, matrix products: 31.8 us -> 8.4 us  [the longest x1 1.71 us: body(): jnp.einsum('qhd,kd->qhk', query_rope, rotated, preferred_element_type=jnp...]
    scatter x2 -> x0, local copies, waits for them, and re-layouts: 7.5 us -> none  [place(): filled = empty.at[target].set(source_rows[token_of])]
    psum x1 -> x0, blocking collectives: 5.67 us -> none  [body(): row_squares = lax.psum(jnp.sum(mixed_wide * mixed_wide, axis=-1), 'tp')]
  transfers between devices with their start and end apart: 4 -> 0, of which waited for: 4 -> 0; matrix products, arithmetic and copies ran while one was open for 5% -> 0% of each run, Pallas kernels for 0% -> 0%
where the time goes in v1:
time: 157 us
  Pallas kernels  134 us (85%)
  other arithmetic  9.43 us (6%)
  matrix products  8.4 us (5%)
  local copies, waits for them, and re-layouts  4.84 us (3%)
    pallas_call x1, Pallas kernels, run_experts(): pl.pallas_call(functools.partial(expert_kernel, n_sp, n_tp), out_shape=ja...  101 us
    pallas_call x1, Pallas kernels, gather_latents(): pl.pallas_call(functools.partial(latent_kernel, n_sp, n_tp), out_shape=ja...  23.9 us
    pallas_call x1, Pallas kernels, project_attended(): pl.pallas_call(functools.partial(attended_kernel, n_sp, n_tp), out_shape=...  8.96 us

profile of v1, /device:TPU:0, one launch (start us, length us, event | category | flops | bytes accessed | tf_op | source)
XLA Modules:
  0.0 157.0 jit_solution(6164734609954027342)
XLA Ops:
  0.0 0.9 copy.69
  0.9 0.1 eq.66
  1.0 1.1 reduce-window.6
  2.2 0.2 slice_reduce_fusion
  2.4 0.1 eq.62
  2.6 0.1 fusion.55
  2.7 0.1 reduce_sum.60
  2.9 0.7 fusion.80
  3.6 0.8 copy.63
  4.5 1.4 fusion.54.block_ref
  5.9 23.9 %gather_latents.1 = bf16[4,4,128,384]{3,2,1,0:T(8,128)(2,1)} custom-call(bf16[64,384]{1,0:T(8,128)(2,1)} %fusion.54.block_ref), custom_call_target="tpu_custom_call" | custom-call | tf_op jit(solution)/shard_map/gather_latents/pallas_call | solution.py:146
  29.9 1.2 slice.71
  31.1 0.2 copy.74
  31.4 0.6 fusion.44
  31.9 0.1 copy.64
  32.1 0.1 multiply_cosine_fusion.1
  32.3 1.6 %fusion.7 = f32[2048]{0:T(1024)S(1)} fusion(bf16[2048,384]{1,0:T(8,128)(2,1)} %bitcast.41), kind=kLoop, calls=%fused_computation.11 | loop fusion | flops 1570816 | bytes 1056768 | tf_op jit(solution)/shard_map/reduce_sum | solution.py:401
  33.9 0.9 convolution_convert_fusion
  34.8 1.3 fusion.23
  36.1 0.5 broadcast_compare_fusion
  36.6 1.7 %fusion.86 = (f32[256,4]{0,1:T(4,128)S(1)}, f32[256,4,2048]{0,2,1:T(8,128)S(1)}) fusion(bf16[2048,16]{0,1:T(8,128)(2,1)S(1)} %get-tuple-element.6, bf16[2048,16]{0,1:T(8,128)(2,1)S(1)} %get-tuple-element.5, bf16[256,4,16]{0,2,1:T(8,128)(2,1)S(1)} %get-tuple-element.8, bf16[256,4,16]{0,2,1:T(8,128)(2,1)S(1)} %get-tuple-element.7, ...), kind=kOutput, calls=%fused_computation.141 | convolution fusion | flops 142998528 | bytes 17502208 | tf_op jit(solution)/shard_map/qhd,kd->qhk/dot_general | solution.py:412
  38.3 1.1 fusion.2
  39.4 1.4 fusion.19
  40.8 0.8 copy.68.att_ref
  41.6 9.0 %project_attended.1 = bf16[256,512]{1,0:T(8,128)(2,1)} custom-call(bf16[256,256]{1,0:T(8,128)(2,1)} %copy.68.att_ref, bf16[1024,512]{1,0:T(8,128)(2,1)} %weight_ref.1, bf16[256,512]{1,0:T(8,128)(2,1)} %resid_ref.1), custom_call_target="tpu_custom_call" | custom-call | tf_op jit(solution)/shard_map/project_attended/pallas_call | solution.py:183
  50.6 0.8 dynamic-slice_convert_fusion
  51.3 1.4 convolution_convert_fusion.1
  52.7 1.1 fusion.32
  53.8 0.2 select_reduce_fusion
  54.1 101.1 %run_experts.1 = bf16[8,128,512]{2,1,0:T(8,128)(2,1)S(1)} custom-call(bf16[8,128,512]{2,1,0:T(8,128)(2,1)S(1)} %bitcast.39, f32[8,8,128]{2,1,0:T(8,128)S(1)} %broadcast_in_dim.36.squares_ref, bf16[1,2048,1024]{2,1,0:T(8,128)(2,1)} %gate_hbm.1, bf16[1,2048,1024]{2,1,0:T(8,128)(2,1)} %up_hbm.1, bf16[1,4096,512]{2,1,0:T(8,128)(2,1)} %down_hbm.1), custom_call_target="tpu_custom_call" | custom-call | tf_op jit(solution)/shard_map/run_experts/pallas_call | solution.py:330
  155.3 0.5 convolution_multiply_fusion
  155.8 1.2 fusion.12
  (33 shorter events, 0.4 us)
Async XLA Ops:
  0.0 33.9 %copy-start = (bf16[256,512]{1,0:T(8,128)(2,1)S(1)}, bf16[256,512]{1,0:T(8,128)(2,1)}, u32[]{:S(2)}) copy-start(bf16[256,512]{1,0:T(8,128)(2,1)} %param.18) | copy-start | bytes 786436
  0.0 31.9 %copy-start.3 = (bf16[256,384]{1,0:T(8,128)(2,1)S(1)}, bf16[256,384]{1,0:T(8,128)(2,1)}, u32[]{:S(2)}) copy-start(bf16[256,384]{1,0:T(8,128)(2,1)} %param.14) | copy-start | bytes 589828
  0.0 32.3 %copy-start.6 = (bf16[256]{0:T(256)(128)(2,1)S(1)}, bf16[256]{0:T(256)(128)(2,1)}, u32[]{:S(2)}) copy-start(bf16[256]{0:T(256)(128)(2,1)} %param.17) | copy-start | bytes 1540
  29.9 4.0 %copy-start.1 = (bf16[4,4,128,384]{3,2,1,0:T(8,128)(2,1)S(1)}, bf16[4,4,128,384]{3,2,1,0:T(8,128)(2,1)}, u32[]{:S(2)}) copy-start(bf16[4,4,128,384]{3,2,1,0:T(8,128)(2,1)} %gather_latents.1) | copy-start | bytes 4718596
  54.1 101.1 %copy-start.4 = (f32[256,2]{0,1:T(2,128)S(1)}, f32[256,2]{0,1:T(2,128)}, u32[]{:S(2)}) copy-start(f32[256,2]{0,1:T(2,128)} %param.23) | copy-start | bytes 6148
  54.1 101.2 %copy-start.5 = (f32[256]{0:T(256)S(1)}, f32[256]{0:T(256)}, u32[]{:S(2)}) copy-start(f32[256]{0:T(256)} %param.24) | copy-start | bytes 3076
  54.1 101.7 %copy-start.2 = (bf16[256,512]{1,0:T(8,128)(2,1)S(1)}, bf16[256,512]{1,0:T(8,128)(2,1)}, u32[]{:S(2)}) copy-start(bf16[256,512]{1,0:T(8,128)(2,1)} %project_attended.1) | copy-start | bytes 786436

commit v2 on v1

--- a/solution.py
+++ b/solution.py
@@ -83,16 +83,17 @@
 
 
 class Spread:
-    def __init__(self, links, bufs, g):
-        self.links, self.bufs, self.g = links, bufs, g
+    def __init__(self, links, bufs, g, source=None):
+        self.links, self.bufs, self.g, self.source = links, bufs, g, source
 
     def start(self):
         ln = self.links
         self.rows, self.twins = [], []
         for buf in self.bufs:
             mine = buf.at[self.g, ln.tp]
-            self.rows.append([ln.send(mine, mine, ln.sp, ln.row(j)) for j in range(1, ln.ny)])
-            self.twins.append(ln.send(mine, mine, ln.sp, ln.twin()))
+            src = mine if self.source is None else self.source
+            self.rows.append([ln.send(src, mine, ln.sp, ln.row(j)) for j in range(1, ln.ny)])
+            self.twins.append(ln.send(src, mine, ln.sp, ln.twin()))
 
     def relay(self):
         ln = self.links
@@ -158,35 +159,44 @@
     )(block)
 
 
-def attended_kernel(n_sp, n_tp, att_ref, weight_ref, resid_ref, mixed_ref, buf, send_sem, recv_sem, local_sem):
+def attended_kernel(n_sp, n_tp, att_ref, weight_ref, resid_ref, mixed_ref, mine, buf, send_sem, recv_sem, local_sem):
     links = Links(n_sp, n_tp, send_sem, recv_sem)
     depth = att_ref.shape[1]
     links.barrier(False)
-    own = pltpu.make_async_copy(att_ref, buf.at[0, links.tp], local_sem)
+    own = pltpu.make_async_copy(att_ref, mine, local_sem)
     own.start()
     own.wait()
-    spread = Spread(links, (buf,), 0)
-    spread.start()
-    spread.relay()
-    spread.finish()
-    total = jnp.zeros(mixed_ref.shape, jnp.float32)
-    for t in range(n_tp):
-        total = total + jnp.dot(
-            buf[0, t], weight_ref[t * depth : (t + 1) * depth, :], preferred_element_type=jnp.float32
-        )
-    mixed_ref[...] = (resid_ref[...].astype(jnp.float32) + total).astype(jnp.bfloat16)
+    half = att_ref.shape[0] // 2
+    spreads = [Spread(links, (buf,), g, mine.at[pl.ds(g * half, half)]) for g in range(2)]
+    for spread in spreads:
+        spread.start()
+    for spread in spreads:
+        spread.relay()
+    for g, spread in enumerate(spreads):
+        spread.finish()
+        buf[g, links.tp] = mine[g * half : (g + 1) * half, :]
+        total = resid_ref[g * half : (g + 1) * half, :].astype(jnp.float32)
+        summed = jnp.zeros(total.shape, jnp.float32)
+        for t in range(n_tp):
+            summed = summed + jnp.dot(
+                buf[g, t],
+                weight_ref[t * depth : (t + 1) * depth, :],
+                preferred_element_type=jnp.float32,
+            )
+        mixed_ref[g * half : (g + 1) * half, :] = (total + summed).astype(jnp.bfloat16)
     links.close()
 
 
 def project_attended(attended, weight, residual, n_sp, n_tp):
-    count = copies_of(n_sp, n_tp, 1, 0, 1)
+    count = copies_of(n_sp, n_tp, 2, 0, 1)
     return pl.pallas_call(
         functools.partial(attended_kernel, n_sp, n_tp),
         out_shape=jax.ShapeDtypeStruct(residual.shape, residual.dtype),
         in_specs=[pl.BlockSpec(memory_space=pltpu.VMEM)] * 3,
         out_specs=pl.BlockSpec(memory_space=pltpu.VMEM),
         scratch_shapes=[
-            pltpu.VMEM((1, n_tp) + attended.shape, attended.dtype),
+            pltpu.VMEM(attended.shape, attended.dtype),
+            pltpu.VMEM((2, n_tp, attended.shape[0] // 2, attended.shape[1]), attended.dtype),
             pltpu.SemaphoreType.DMA((count,)),
             pltpu.SemaphoreType.DMA((count,)),
             pltpu.SemaphoreType.DMA,
@@ -197,13 +207,15 @@
 
 
 def expert_kernel(
-    n_sp, n_tp, placed_ref, squares_ref, gate_hbm, up_hbm, down_hbm, ret_ref,
-    rx, sq, hid, ostage, gate_w, up_w, down_w, send_sem, recv_sem, local_sem,
+    n_sp, n_tp, placed_ref, squares_ref, gate_hbm, up_hbm, down_hbm, across_hbm, ret_ref,
+    rx, sq, hid, own_sum, part_out, part_in, ostage,
+    gate_w, up_w, down_w, across_w, send_sem, recv_sem, local_sem,
 ):
     cap, width = placed_ref.shape[1:]
     per = n_sp // GROUPS
     d_model = width * n_tp
     hidden_here = gate_w.shape[1]
+    deep = 2 * hidden_here
     links = Links(n_sp, n_tp, send_sem, recv_sem)
     links.barrier(True)
     own = pltpu.make_async_copy(placed_ref.at[0], rx.at[0, links.tp, pl.ds(0, cap)], local_sem.at[0])
@@ -221,12 +233,16 @@
     loads = [
         pltpu.make_async_copy(gate_hbm.at[0], gate_w, local_sem.at[2]),
         pltpu.make_async_copy(up_hbm.at[0], up_w, local_sem.at[3]),
-        pltpu.make_async_copy(down_hbm.at[0], down_w, local_sem.at[4]),
+        pltpu.make_async_copy(across_hbm, across_w, local_sem.at[4]),
+        pltpu.make_async_copy(
+            down_hbm.at[0, pl.ds(pl.multiple_of(links.y * deep, 128), deep)], down_w, local_sem.at[6]
+        ),
     ]
     for load in loads:
         load.start()
     inputs = [Spread(links, (sq, rx), g) for g in range(GROUPS)]
-    hiddens = [Spread(links, (hid,), g) for g in range(GROUPS)]
+    twins = {}
+    parts = {}
     returning = []
 
     def arrive(g):
@@ -269,29 +285,54 @@
             gate = gate * scale
             upper = upper * scale
             value = gate / (1.0 + jnp.exp(-gate)) * upper
-            hid[g, links.tp, :, cols] = value.astype(jnp.bfloat16)
-
-        hiddens[g].start()
+            hid[g, links.core, :, cols] = value.astype(jnp.bfloat16)
+
+        half = hid.at[g, links.core]
+        twins[g] = links.send(half, half, links.sp, links.twin())
+
+    tile_out = min(256, width)
+
+    def product(g, weight, cols):
+        total = jnp.zeros((per * cap, tile_out), jnp.float32)
+        for c in range(2):
+            total = total + jnp.dot(
+                hid[g, c],
+                weight[pl.ds(c * hidden_here, hidden_here), cols],
+                preferred_element_type=jnp.float32,
+            )
+        return total
 
     def down_stage(g):
-        hiddens[g].relay()
-        hiddens[g].finish()
+        twins[g].wait_recv()
         if g == 0:
             loads[2].wait()
-        tile = min(256, width)
-
-        @pl.loop(0, width // tile)
+        parts[g] = []
+        for j in range(1, links.ny):
+
+            @pl.loop(0, width // tile_out)
+            def _(n):
+                cols = pl.ds(pl.multiple_of(n * tile_out, tile_out), tile_out)
+                part_out[g, j - 1, :, cols] = product(g, across_w.at[j - 1], cols).astype(
+                    jnp.bfloat16
+                )
+
+            parts[g].append(
+                links.send(part_out.at[g, j - 1], part_in.at[g, j - 1], links.sp, links.row(j))
+            )
+        if g == 0:
+            loads[3].wait()
+
+        @pl.loop(0, width // tile_out)
         def _(n):
-            cols = pl.ds(pl.multiple_of(n * tile, tile), tile)
-            total = jnp.zeros((per * cap, tile), jnp.float32)
-            for t in range(n_tp):
-                total = total + jnp.dot(
-                    hid[g, t],
-                    down_w[pl.ds(t * hidden_here, hidden_here), cols],
-                    preferred_element_type=jnp.float32,
-                )
-            ostage[g, :, cols] = total.astype(jnp.bfloat16)
-
+            cols = pl.ds(pl.multiple_of(n * tile_out, tile_out), tile_out)
+            own_sum[g, :, cols] = product(g, down_w, cols)
+
+    def return_stage(g):
+        total = own_sum[g]
+        for j, copy in enumerate(parts[g]):
+            copy.wait_recv()
+            total = total + part_in[g, j].astype(jnp.float32)
+        ostage[g] = total.astype(jnp.bfloat16)
         for i in range(per):
             r = g * per + i
             piece = ostage.at[g, pl.ds(i * cap, cap)]
@@ -310,45 +351,53 @@
     for g in range(2, GROUPS):
         arrive(g)
         up_stage(g - 1)
-    down_stage(0)
+        down_stage(g - 2)
     up_stage(GROUPS - 1)
+    down_stage(GROUPS - 2)
+    return_stage(0)
+    down_stage(GROUPS - 1)
     for g in range(1, GROUPS):
-        down_stage(g)
+        return_stage(g)
     returning[0].wait()
     for copy in returning[1:]:
         copy.wait_recv()
     links.close()
 
 
-def run_experts(placed, squares, gate_weight, up_weight, down_weight, n_sp, n_tp):
+def run_experts(placed, squares, gate_weight, up_weight, down_weight, across, n_sp, n_tp):
     cap, width = placed.shape[1:]
     per = n_sp // GROUPS
     hidden_here = gate_weight.shape[2]
-    count = copies_of(n_sp, n_tp, GROUPS, 3, 3)
+    ny = n_tp // 2
+    count = copies_of(n_sp, n_tp, GROUPS, 3, 2) + GROUPS * ny
     vmem = pl.BlockSpec(memory_space=pltpu.VMEM)
     hbm = pl.BlockSpec(memory_space=pl.ANY)
     return pl.pallas_call(
         functools.partial(expert_kernel, n_sp, n_tp),
         out_shape=jax.ShapeDtypeStruct(placed.shape, placed.dtype),
-        in_specs=[vmem, vmem, hbm, hbm, hbm],
+        in_specs=[vmem, vmem, hbm, hbm, hbm, hbm],
         out_specs=vmem,
         scratch_shapes=[
             pltpu.VMEM((GROUPS, n_tp, per * cap, width), jnp.bfloat16),
             pltpu.VMEM((GROUPS, n_tp, per) + squares.shape[1:], jnp.float32),
-            pltpu.VMEM((GROUPS, n_tp, per * cap, hidden_here), jnp.bfloat16),
+            pltpu.VMEM((GROUPS, 2, per * cap, hidden_here), jnp.bfloat16),
+            pltpu.VMEM((GROUPS, per * cap, width), jnp.float32),
+            pltpu.VMEM((GROUPS, ny - 1, per * cap, width), jnp.bfloat16),
+            pltpu.VMEM((GROUPS, ny - 1, per * cap, width), jnp.bfloat16),
             pltpu.VMEM((GROUPS, per * cap, width), jnp.bfloat16),
             pltpu.VMEM(gate_weight.shape[1:], jnp.bfloat16),
             pltpu.VMEM(up_weight.shape[1:], jnp.bfloat16),
-            pltpu.VMEM(down_weight.shape[1:], jnp.bfloat16),
+            pltpu.VMEM((2 * hidden_here, width), jnp.bfloat16),
+            pltpu.VMEM(across.shape, jnp.bfloat16),
             pltpu.SemaphoreType.DMA((count,)),
             pltpu.SemaphoreType.DMA((count,)),
-            pltpu.SemaphoreType.DMA((6,)),
+            pltpu.SemaphoreType.DMA((7,)),
         ],
         compiler_params=pltpu.CompilerParams(
             collective_id=2, has_side_effects=True, vmem_limit_bytes=50 * 1024 * 1024
         ),
         name="run_experts",
-    )(placed, squares, gate_weight, up_weight, down_weight)
+    )(placed, squares, gate_weight, up_weight, down_weight, across)
 
 
 def body(
@@ -375,14 +424,31 @@
     length = n_sp * tokens_here
     quarter = tokens_here // n_tp
 
-    pad = -(rank + ROPE) % LANES
+    ny, deep = n_tp // 2, 2 * gate_weight.shape[2]
+    across = []
+    for j in range(1, ny):
+        there = (tp // 2 + j) % ny
+        rows = lax.dynamic_slice_in_dim(down_weight[0], there * deep, deep, 0)
+        pairs = [(t, (t // 2 + j) % ny * 2 + t % 2) for t in range(n_tp)]
+        across.append(lax.ppermute(rows, "tp", pairs))
+    across = across[::-1]
+
+    rope_rows = -(-quarter * ROPE // rank)
+    pad = -rope_rows % 8
+    rope_part = lax.dynamic_slice_in_dim(rope_key, tp * quarter, quarter, 0)
     block = jnp.concatenate(
-        [latent, rope_key, jnp.zeros((tokens_here, pad), latent.dtype)], axis=1
-    )
-    block = lax.dynamic_slice_in_dim(block, tp * quarter, quarter, 0)
+        [
+            lax.dynamic_slice_in_dim(latent, tp * quarter, quarter, 0),
+            rope_part.reshape(rope_rows, rank),
+            jnp.zeros((pad, rank), latent.dtype),
+        ],
+        axis=0,
+    )
     per = n_sp // GROUPS
     gathered = gather_latents(block, n_sp, n_tp)
-    gathered = gathered.reshape(length, rank + ROPE + pad)
+    gathered = gathered.reshape(n_sp * n_tp, quarter + rope_rows + pad, rank)
+    latent_all = gathered[:, :quarter].reshape(length, rank)
+    rope_all = gathered[:, quarter : quarter + rope_rows].reshape(length, ROPE)
     index = jnp.arange(length, dtype=jnp.int32)
     in_quarter = index % quarter
     in_group = index // quarter % per
@@ -396,7 +462,7 @@
     query_nope = query[..., :NOPE]
     query_rope = rotate(query[..., NOPE:], positions).astype(jnp.bfloat16)
     scaling = (NOPE + ROPE) ** (-0.5)
-    latent_wide = gathered[:, :rank].astype(jnp.float32)
+    latent_wide = latent_all.astype(jnp.float32)
     normed = latent_wide * lax.rsqrt(
         jnp.mean(latent_wide * latent_wide, axis=-1, keepdims=True) + EPSILON
     )
@@ -404,7 +470,7 @@
     key_value = jnp.dot(normed, key_value_weight, preferred_element_type=jnp.float32).astype(
         jnp.bfloat16
     )
-    rotated = rotate(gathered[:, rank : rank + ROPE], key_positions).astype(jnp.bfloat16)
+    rotated = rotate(rope_all, key_positions).astype(jnp.bfloat16)
     key_value = key_value.reshape(length, heads_here, NOPE + VDIM)
     scores = jnp.einsum(
         "qhd,khd->qhk", query_nope, key_value[..., :NOPE], preferred_element_type=jnp.float32
@@ -460,6 +526,7 @@
         gate_weight,
         up_weight,
         down_weight,
+        jnp.stack(across),
         n_sp,
         n_tp,
     ).reshape(n_sp * capacity, width_here)

time: 157 us -> 180 us (1.15); the launches traced: 157 us -> 176 us
  local copies, waits for them, and re-layouts: 4.84 us -> 12.9 us
  Pallas kernels: 134 us -> 142 us
  starting transfers between devices: 0 us -> 3 us
    pallas_call x1, Pallas kernels: 23.9 us -> 54.7 us  [gather_latents(): pl.pallas_call(functools.partial(latent_kernel, n_sp, n_tp), out_shape=ja...]
    pallas_call x1, Pallas kernels: 101 us -> 77.9 us  [run_experts(): pl.pallas_call(functools.partial(expert_kernel, n_sp, n_tp), out_shape=ja...]
    dynamic_slice x0 -> x4, local copies, waits for them, and re-layouts: none -> 4.07 us  [the longest x1 3.13 us: body(): rows = lax.dynamic_slice_in_dim(down_weight[0], there * deep, deep, 0)]
    ppermute x0 -> x1, starting transfers between devices: none -> 3 us  [body(): across.append(lax.ppermute(rows, 'tp', pairs))]
    unnamed x18 -> x20, local copies, waits for them, and re-layouts: 2.06 us -> 4.29 us
  transfers between devices with their start and end apart: 0 -> 1, of which waited for: 0 -> 0; matrix products, arithmetic and copies ran while one was open for 0% -> 15% of each run, Pallas kernels for 0% -> 36%
where the time goes in v2:
time: 180 us; the launch traced here: 176 us
  Pallas kernels  142 us (79%)
  local copies, waits for them, and re-layouts  12.9 us (7%)
  other arithmetic  10.2 us (6%)
  matrix products  8.28 us (5%)
  starting transfers between devices  3 us (2%)
    pallas_call x1, Pallas kernels, run_experts(): pl.pallas_call(functools.partial(expert_kernel, n_sp, n_tp), out_shape=ja...  77.9 us
    pallas_call x1, Pallas kernels, gather_latents(): pl.pallas_call(functools.partial(latent_kernel, n_sp, n_tp), out_shape=ja...  54.7 us
    pallas_call x1, Pallas kernels, project_attended(): pl.pallas_call(functools.partial(attended_kernel, n_sp, n_tp), out_shape=...  8.95 us
    unnamed x20, local copies, waits for them, and re-layouts  4.29 us
  transfers between devices with their start and end apart: 1, of which 0 were waited for; matrix products, arithmetic and copies ran while one was open for 15% of the time, Pallas kernels for 36%

profile of v2, /device:TPU:0, one launch (start us, length us, event | category | flops | bytes accessed | tf_op | source)
XLA Modules:
  0.0 176.4 jit_solution(18013651981998514129)
XLA Ops:
  0.0 3.1 %dynamic-slice_bitcast_fusion = bf16[2048,512]{1,0:T(8,128)(2,1)} fusion(bf16[1,4096,512]{2,1,0:T(8,128)(2,1)} %down_hbm.1, s32[]{:T(128)S(6)} %select_n.153), kind=kLoop, calls=%fused_computation.12 | loop fusion | bytes 4194308 | tf_op jit(solution)/shard_map/dynamic_slice | solution.py:431
  3.1 3.0 %collective-permute-start = (bf16[2048,512]{1,0:T(8,128)(2,1)}, bf16[2048,512]{1,0:T(8,128)(2,1)}, u32[]{:S(2)}, u32[]{:S(2)}) collective-permute-start(bf16[2048,512]{1,0:T(8,128)(2,1)} %dynamic-slice_bitcast_fusion), channel_id=1, source_target_pairs={{0,2},{1,3},{2,0},{3,1},{4,6},{5,7},{6,4},{7,5},{8,10},{9,11},{10,... | collective-permute-start | bytes 6291464 | tf_op jit(solution)/shard_map/ppermute | solution.py:433
  6.1 0.8 constant_dynamic-slice_fusion.1
  7.2 0.6 pad_maximum_fusion.block_ref
  7.8 54.7 %gather_latents.1 = bf16[4,4,144,256]{3,2,1,0:T(8,128)(2,1)} custom-call(bf16[72,256]{1,0:T(8,128)(2,1)} %pad_maximum_fusion.block_ref), custom_call_target="tpu_custom_call" | custom-call | tf_op jit(solution)/shard_map/gather_latents/pallas_call | solution.py:147
  62.6 1.7 slice_convert_fusion.1
  64.3 1.5 slice_convert_fusion
  65.8 0.3 multiply_reduce_fusion
  66.2 1.2 reshape.355
  67.4 1.7 fusion.77
  69.1 1.5 copy.77
  70.6 1.5 copy.78
  72.2 1.1 copy.66
  73.3 0.3 fusion.8
  73.7 0.8 convolution_convert_fusion
  74.4 1.3 fusion.21
  75.9 0.5 broadcast_compare_fusion
  76.4 0.6 fusion.39
  77.0 1.7 fusion.80
  78.7 1.1 fusion.2
  79.8 1.4 fusion.18
  81.7 0.8 copy.71.att_ref
  82.4 1.1 reduce-window.6
  83.6 0.2 slice_reduce_fusion
  84.2 9.0 %project_attended.1 = bf16[256,512]{1,0:T(8,128)(2,1)} custom-call(bf16[256,256]{1,0:T(8,128)(2,1)} %copy.71.att_ref, bf16[1024,512]{1,0:T(8,128)(2,1)} %weight_ref.1, bf16[256,512]{1,0:T(8,128)(2,1)} %resid_ref.1), custom_call_target="tpu_custom_call" | custom-call | tf_op jit(solution)/shard_map/project_attended/pallas_call | solution.py:192
  93.1 0.8 dynamic-slice_convert_fusion
  93.9 1.1 fusion.27
  95.0 0.2 select_reduce_fusion
  95.3 1.4 convolution_convert_fusion.1
  96.7 77.9 %run_experts.1 = bf16[8,128,512]{2,1,0:T(8,128)(2,1)S(1)} custom-call(bf16[8,128,512]{2,1,0:T(8,128)(2,1)S(1)} %bitcast.49, f32[8,8,128]{2,1,0:T(8,128)S(1)} %broadcast_in_dim.33.squares_ref, bf16[1,2048,1024]{2,1,0:T(8,128)(2,1)} %gate_hbm.1, bf16[1,2048,1024]{2,1,0:T(8,128)(2,1)} %up_hbm.1, bf16[1,4096,512]{2,1,0:T(8,128)(2,1)} %down_hbm.1, ...), custom_call_target="tpu_custom_call" | custom-call | tf_op jit(solution)/shard_map/run_experts/pallas_call | solution.py:375
  174.7 0.5 convolution_multiply_fusion
  175.2 1.2 fusion.11
  (44 shorter events, 1.5 us)
Async XLA Ops:
  0.0 73.6 %copy-start = (bf16[256,512]{1,0:T(8,128)(2,1)S(1)}, bf16[256,512]{1,0:T(8,128)(2,1)}, u32[]{:S(2)}) copy-start(bf16[256,512]{1,0:T(8,128)(2,1)} %param.18) | copy-start | bytes 786436
  0.0 6.9 %copy-start.5 = (bf16[256,32]{0,1:T(8,128)(2,1)S(1)}, bf16[256,32]{0,1:T(8,128)(2,1)}, u32[]{:S(2)}) copy-start(bf16[256,32]{0,1:T(8,128)(2,1)} %param.16) | copy-start | bytes 49156
  3.1 93.5 %collective-permute-start = (bf16[2048,512]{1,0:T(8,128)(2,1)}, bf16[2048,512]{1,0:T(8,128)(2,1)}, u32[]{:S(2)}, u32[]{:S(2)}) collective-permute-start(bf16[2048,512]{1,0:T(8,128)(2,1)} %dynamic-slice_bitcast_fusion), channel_id=1, source_target_pairs={{0,2},{1,3},{2,0},{3,1},{4,6},{5,7},{6,4},{7,5},{8,10},{9,11},{10,... | collective-permute-start | bytes 6291464 | tf_op jit(solution)/shard_map/ppermute | solution.py:433
  62.6 3.2 %copy-start.1 = (bf16[4,4,144,256]{3,2,1,0:T(8,128)(2,1)S(1)}, bf16[4,4,144,256]{3,2,1,0:T(8,128)(2,1)}, u32[]{:S(2)}) copy-start(bf16[4,4,144,256]{3,2,1,0:T(8,128)(2,1)} %gather_latents.1) | copy-start | bytes 3538948
  66.1 6.1 %copy-start.7 = (bf16[256]{0:T(256)(128)(2,1)S(1)}, bf16[256]{0:T(256)(128)(2,1)}, u32[]{:S(2)}) copy-start(bf16[256]{0:T(256)(128)(2,1)} %param.17) | copy-start | bytes 1540
  79.8 1.4 copy-start.3
  79.8 4.3 %copy-start.4 = (f32[256,2]{0,1:T(2,128)S(1)}, f32[256,2]{0,1:T(2,128)}, u32[]{:S(2)}) copy-start(f32[256,2]{0,1:T(2,128)} %param.23) | copy-start | bytes 6148
  79.8 15.4 %copy-start.6 = (f32[256]{0:T(256)S(1)}, f32[256]{0:T(256)}, u32[]{:S(2)}) copy-start(f32[256]{0:T(256)} %param.24) | copy-start | bytes 3076
  96.7 78.5 %copy-start.2 = (bf16[256,512]{1,0:T(8,128)(2,1)S(1)}, bf16[256,512]{1,0:T(8,128)(2,1)}, u32[]{:S(2)}) copy-start(bf16[256,512]{1,0:T(8,128)(2,1)} %project_attended.1) | copy-start | bytes 786436

commit v3 on v2

--- a/solution.py
+++ b/solution.py
@@ -117,14 +117,14 @@
     per = n_sp // GROUPS
     links = Links(n_sp, n_tp, send_sem, recv_sem)
     links.barrier(True)
-    own = pltpu.make_async_copy(block_ref, buf.at[0, links.tp, pl.ds(0, rows)], local_sem)
+    own = pltpu.make_async_copy(block_ref, buf.at[0, links.core, pl.ds(0, rows)], local_sem)
     own.start()
     arriving = [own]
     for r in range(1, n_sp):
         g, i = divmod(r, per)
-        dst = buf.at[g, links.tp, pl.ds(i * rows, rows)]
+        dst = buf.at[g, links.core, pl.ds(i * rows, rows)]
         arriving.append(links.send(block_ref, dst, (links.sp + n_sp - r) % n_sp, links.tp))
-    spreads = [Spread(links, (buf,), g) for g in range(GROUPS)]
+    twins = []
     for g in range(GROUPS):
         for i in range(per):
             r = g * per + i
@@ -132,21 +132,19 @@
                 own.wait()
             else:
                 arriving[r].wait_recv()
-        spreads[g].start()
-        if g > 0:
-            spreads[g - 1].relay()
-    spreads[-1].relay()
-    for spread in spreads:
-        spread.finish()
+        half = buf.at[g, links.core]
+        twins.append(links.send(half, half, links.sp, links.twin()))
+    for copy in twins:
+        copy.wait_recv()
     links.close()
 
 
 def gather_latents(block, n_sp, n_tp):
     rows, width = block.shape
-    count = copies_of(n_sp, n_tp, GROUPS, 1, 1)
+    count = n_sp - 1 + GROUPS
     return pl.pallas_call(
         functools.partial(latent_kernel, n_sp, n_tp),
-        out_shape=jax.ShapeDtypeStruct((GROUPS, n_tp, n_sp // GROUPS * rows, width), block.dtype),
+        out_shape=jax.ShapeDtypeStruct((GROUPS, 2, n_sp // GROUPS * rows, width), block.dtype),
         in_specs=[pl.BlockSpec(memory_space=pltpu.VMEM)],
         out_specs=pl.BlockSpec(memory_space=pltpu.VMEM),
         scratch_shapes=[
@@ -422,7 +420,7 @@
     heads_here = key_value_weight.shape[1] // (NOPE + VDIM)
     width_here = residual.shape[1]
     length = n_sp * tokens_here
-    quarter = tokens_here // n_tp
+    part = tokens_here // 2
 
     ny, deep = n_tp // 2, 2 * gate_weight.shape[2]
     across = []
@@ -433,36 +431,28 @@
         across.append(lax.ppermute(rows, "tp", pairs))
     across = across[::-1]
 
-    rope_rows = -(-quarter * ROPE // rank)
-    pad = -rope_rows % 8
-    rope_part = lax.dynamic_slice_in_dim(rope_key, tp * quarter, quarter, 0)
+    pad = -(rank + ROPE) % LANES
     block = jnp.concatenate(
-        [
-            lax.dynamic_slice_in_dim(latent, tp * quarter, quarter, 0),
-            rope_part.reshape(rope_rows, rank),
-            jnp.zeros((pad, rank), latent.dtype),
-        ],
-        axis=0,
-    )
+        [latent, rope_key, jnp.zeros((tokens_here, pad), latent.dtype)], axis=1
+    )
+    block = lax.dynamic_slice_in_dim(block, tp % 2 * part, part, 0)
     per = n_sp // GROUPS
     gathered = gather_latents(block, n_sp, n_tp)
-    gathered = gathered.reshape(n_sp * n_tp, quarter + rope_rows + pad, rank)
-    latent_all = gathered[:, :quarter].reshape(length, rank)
-    rope_all = gathered[:, quarter : quarter + rope_rows].reshape(length, ROPE)
+    gathered = gathered.reshape(length, rank + ROPE + pad)
     index = jnp.arange(length, dtype=jnp.int32)
-    in_quarter = index % quarter
-    in_group = index // quarter % per
-    of_tp = index // (quarter * per) % n_tp
-    group = index // (quarter * per * n_tp)
+    in_part = index % part
+    in_group = index // part % per
+    of_core = index // (part * per) % 2
+    group = index // (part * per * 2)
     source = (sp + group * per + in_group) % n_sp
-    key_positions = source * tokens_here + of_tp * quarter + in_quarter
+    key_positions = source * tokens_here + of_core * part + in_part
 
     positions = sp * tokens_here + jnp.arange(tokens_here, dtype=jnp.int32)
     query = queries.reshape(tokens_here, heads_here, NOPE + ROPE)
     query_nope = query[..., :NOPE]
     query_rope = rotate(query[..., NOPE:], positions).astype(jnp.bfloat16)
     scaling = (NOPE + ROPE) ** (-0.5)
-    latent_wide = latent_all.astype(jnp.float32)
+    latent_wide = gathered[:, :rank].astype(jnp.float32)
     normed = latent_wide * lax.rsqrt(
         jnp.mean(latent_wide * latent_wide, axis=-1, keepdims=True) + EPSILON
     )
@@ -470,7 +460,7 @@
     key_value = jnp.dot(normed, key_value_weight, preferred_element_type=jnp.float32).astype(
         jnp.bfloat16
     )
-    rotated = rotate(rope_all, key_positions).astype(jnp.bfloat16)
+    rotated = rotate(gathered[:, rank : rank + ROPE], key_positions).astype(jnp.bfloat16)
     key_value = key_value.reshape(length, heads_here, NOPE + VDIM)
     scores = jnp.einsum(
         "qhd,khd->qhk", query_nope, key_value[..., :NOPE], preferred_element_type=jnp.float32

time: 180 us -> 143 us (0.79); the launches traced: 176 us -> 142 us
  Pallas kernels: 142 us -> 110 us
  local copies, waits for them, and re-layouts: 12.9 us -> 7.19 us
  matrix products: 8.28 us -> 13.3 us
  other arithmetic: 10.2 us -> 8.01 us
    pallas_call x1, Pallas kernels: 54.7 us -> 25.8 us  [gather_latents(): pl.pallas_call(functools.partial(latent_kernel, n_sp, n_tp), out_shape=ja...]
    dot_general x1, matrix products: 1.4 us -> 5.15 us  [body(): jnp.einsum('qhk,khd->qhd', exp_scores.astype(jnp.bfloat16), key_value[......]
    pallas_call x1, Pallas kernels: 77.9 us -> 75.6 us  [run_experts(): pl.pallas_call(functools.partial(expert_kernel, n_sp, n_tp), out_shape=ja...]
    unnamed x20 -> x28, local copies, waits for them, and re-layouts: 4.29 us -> 2.72 us
  transfers between devices with their start and end apart: 1 -> 1, of which waited for: 0 -> 0; matrix products, arithmetic and copies ran while one was open for 15% -> 16% of each run, Pallas kernels for 36% -> 24%
where the time goes in v3:
time: 143 us; the launch traced here: 142 us
  Pallas kernels  110 us (77%)
  matrix products  13.3 us (9%)
  other arithmetic  8.01 us (6%)
  local copies, waits for them, and re-layouts  7.19 us (5%)
  starting transfers between devices  3.08 us (2%)
    pallas_call x1, Pallas kernels, run_experts(): pl.pallas_call(functools.partial(expert_kernel, n_sp, n_tp), out_shape=ja...  75.6 us
    pallas_call x1, Pallas kernels, gather_latents(): pl.pallas_call(functools.partial(latent_kernel, n_sp, n_tp), out_shape=ja...  25.8 us
    pallas_call x1, Pallas kernels, project_attended(): pl.pallas_call(functools.partial(attended_kernel, n_sp, n_tp), out_shape=...  8.95 us
    dot_general x1, matrix products, body(): jnp.einsum('qhk,khd->qhd', exp_scores.astype(jnp.bfloat16), key_value[......  5.15 us
    ppermute x1, starting transfers between devices, body(): across.append(lax.ppermute(rows, 'tp', pairs))  3.08 us
  transfers between devices with their start and end apart: 1, of which 0 were waited for; matrix products, arithmetic and copies ran while one was open for 16% of the time, Pallas kernels for 24%

profile of v3, /device:TPU:0, one launch (start us, length us, event | category | flops | bytes accessed | tf_op | source)
XLA Modules:
  0.0 142.4 jit_solution(14778767249077570954)
XLA Ops:
  0.1 1.8 %dynamic-slice_bitcast_fusion = bf16[2048,512]{1,0:T(8,128)(2,1)S(1)} fusion(bf16[1,4096,512]{2,1,0:T(8,128)(2,1)} %down_hbm.1, s32[]{:T(128)S(6)} %select_n.157), kind=kLoop, calls=%fused_computation.14 | loop fusion | bytes 4194308 | tf_op jit(solution)/shard_map/dynamic_slice | solution.py:429
  1.9 3.1 %collective-permute-start = (bf16[2048,512]{1,0:T(8,128)(2,1)S(1)}, bf16[2048,512]{1,0:T(8,128)(2,1)}, u32[]{:S(2)}, u32[]{:S(2)}) collective-permute-start(bf16[2048,512]{1,0:T(8,128)(2,1)S(1)} %dynamic-slice_bitcast_fusion), channel_id=1, source_target_pairs={{0,2},{1,3},{2,0},{3,1},{4,6},{5,7},{6,4},{7,5},{8,10},{9,11},{10,... | collective-permute-start | bytes 6291464 | tf_op jit(solution)/shard_map/ppermute | solution.py:431
  5.0 0.1 copy.69
  5.1 0.1 eq.69
  5.3 0.1 eq.65
  5.7 0.7 fusion.51.block_ref
  6.4 25.8 %gather_latents.1 = bf16[4,2,256,384]{3,2,1,0:T(8,128)(2,1)} custom-call(bf16[128,384]{1,0:T(8,128)(2,1)} %fusion.51.block_ref), custom_call_target="tpu_custom_call" | custom-call | tf_op jit(solution)/shard_map/gather_latents/pallas_call | solution.py:145
  32.1 1.1 slice.71
  33.2 1.6 %fusion.7 = f32[2048]{0:T(1024)S(1)} fusion(bf16[2048,384]{1,0:T(8,128)(2,1)} %bitcast.44), kind=kLoop, calls=%fused_computation.11 | loop fusion | flops 1570816 | bytes 1056768 | tf_op jit(solution)/shard_map/reduce_sum | solution.py:457
  34.8 1.1 reduce-window.6
  35.9 0.2 slice_reduce_fusion
  36.2 0.2 copy.74
  36.4 0.1 copy.64
  36.7 2.1 %convolution_convert_fusion = bf16[2048,512]{0,1:T(8,128)(2,1)S(1)} fusion(bf16[256,512]{1,0:T(8,128)(2,1)S(1)} %copy-done, f32[256]{0:T(256)S(1)} %convert_element_type.64, f32[2048]{0:T(1024)S(1)} %add_rsqrt_fusion, bf16[2048,384]{1,0:T(8,128)(2,1)} %bitcast.45), kind=kOutput, calls=%fused_computation.8 | convolution fusion | flops 540016640 | bytes 3417088 | tf_op jit(solution)/shard_map/dot_general | solution.py:460
  38.8 1.3 fusion.23
  40.1 0.1 multiply_cosine_fusion.1
  40.2 0.6 fusion.44
  40.8 0.5 broadcast_compare_fusion
  41.3 1.7 %fusion.86 = (f32[256,4]{0,1:T(4,128)S(1)}, f32[256,4,2048]{0,2,1:T(8,128)S(1)}) fusion(bf16[2048,16]{0,1:T(8,128)(2,1)S(1)} %get-tuple-element.6, bf16[2048,16]{0,1:T(8,128)(2,1)S(1)} %get-tuple-element.5, bf16[256,4,16]{0,2,1:T(8,128)(2,1)S(1)} %get-tuple-element.8, bf16[256,4,16]{0,2,1:T(8,128)(2,1)S(1)} %get-tuple-element.7, ...), kind=kOutput, calls=%fused_computation.142 | convolution fusion | flops 142998528 | bytes 17502208 | tf_op jit(solution)/shard_map/qhd,kd->qhk/dot_general | solution.py:468
  43.0 1.1 fusion.2
  44.1 2.1 %copy-done.1 = f32[256,4,2048]{0,2,1:T(8,128)} copy-done((f32[256,4,2048]{0,2,1:T(8,128)}, f32[256,4,2048]{0,2,1:T(8,128)S(1)}, u32[]{:S(2)}) %copy-start.1) | copy-done | bytes 8388632
  46.3 0.1 reduce_sum.60
  46.5 5.2 %fusion.19 = bf16[256,4,64]{0,2,1:T(8,128)(2,1)S(1)} fusion(f32[256,4,2048]{0,2,1:T(8,128)} %copy-done.1, f32[256,4]{0,1:T(4,128)S(1)} %get-tuple-element.15, bf16[2048,4,128]{0,2,1:T(8,128)(2,1)} %bitcast.47, f32[256,4]{0,1:T(4,128)S(1)} %fusion.2), kind=kOutput, calls=%fused_computation.23 | convolution fusion | flops 272760832 | bytes 9576448 | tf_op jit(solution)/shard_map/qhk,khd->qhd/dot_general | solution.py:477
  51.7 0.8 copy.68.att_ref
  52.5 9.0 %project_attended.1 = bf16[256,512]{1,0:T(8,128)(2,1)} custom-call(bf16[256,256]{1,0:T(8,128)(2,1)} %copy.68.att_ref, bf16[1024,512]{1,0:T(8,128)(2,1)} %weight_ref.1, bf16[256,512]{1,0:T(8,128)(2,1)} %resid_ref.1), custom_call_target="tpu_custom_call" | custom-call | tf_op jit(solution)/shard_map/project_attended/pallas_call | solution.py:190
  61.4 0.8 dynamic-slice_convert_fusion
  62.2 1.1 fusion.32
  63.3 0.2 select_reduce_fusion
  63.6 1.4 convolution_convert_fusion.1
  65.0 75.6 %run_experts.1 = bf16[8,128,512]{2,1,0:T(8,128)(2,1)S(1)} custom-call(bf16[8,128,512]{2,1,0:T(8,128)(2,1)S(1)} %bitcast.42, f32[8,8,128]{2,1,0:T(8,128)S(1)} %broadcast_in_dim.36.squares_ref, bf16[1,2048,1024]{2,1,0:T(8,128)(2,1)} %gate_hbm.1, bf16[1,2048,1024]{2,1,0:T(8,128)(2,1)} %up_hbm.1, bf16[1,4096,512]{2,1,0:T(8,128)(2,1)} %down_hbm.1, ...), custom_call_target="tpu_custom_call" | custom-call | tf_op jit(solution)/shard_map/run_experts/pallas_call | solution.py:373
  140.7 0.5 convolution_multiply_fusion
  141.2 1.2 fusion.12
  (47 shorter events, 0.6 us)
Async XLA Ops:
  0.0 36.7 %copy-start = (bf16[256,512]{1,0:T(8,128)(2,1)S(1)}, bf16[256,512]{1,0:T(8,128)(2,1)}, u32[]{:S(2)}) copy-start(bf16[256,512]{1,0:T(8,128)(2,1)} %param.18) | copy-start | bytes 786436
  0.0 5.0 %copy-start.8 = (s32[256,2]{0,1:T(2,128)S(1)}, s32[256,2]{0,1:T(2,128)}, u32[]{:S(2)}) copy-start(s32[256,2]{0,1:T(2,128)} %param.22) | copy-start | bytes 6148
  0.0 5.5 %copy-start.6 = (bf16[256,32]{0,1:T(8,128)(2,1)S(1)}, bf16[256,32]{0,1:T(8,128)(2,1)}, u32[]{:S(2)}) copy-start(bf16[256,32]{0,1:T(8,128)(2,1)} %param.16) | copy-start | bytes 49156
  0.0 5.7 %copy-start.5 = (bf16[256,256]{1,0:T(8,128)(2,1)S(1)}, bf16[256,256]{1,0:T(8,128)(2,1)}, u32[]{:S(2)}) copy-start(bf16[256,256]{1,0:T(8,128)(2,1)} %param.15) | copy-start | bytes 393220
  0.0 36.4 %copy-start.4 = (bf16[256,384]{1,0:T(8,128)(2,1)S(1)}, bf16[256,384]{1,0:T(8,128)(2,1)}, u32[]{:S(2)}) copy-start(bf16[256,384]{1,0:T(8,128)(2,1)} %param.14) | copy-start | bytes 589828
  1.9 34.7 %copy-start.11 = (bf16[256]{0:T(256)(128)(2,1)S(1)}, bf16[256]{0:T(256)(128)(2,1)}, u32[]{:S(2)}) copy-start(bf16[256]{0:T(256)(128)(2,1)} %param.17) | copy-start | bytes 1540
  1.9 63.1 %collective-permute-start = (bf16[2048,512]{1,0:T(8,128)(2,1)S(1)}, bf16[2048,512]{1,0:T(8,128)(2,1)}, u32[]{:S(2)}, u32[]{:S(2)}) collective-permute-start(bf16[2048,512]{1,0:T(8,128)(2,1)S(1)} %dynamic-slice_bitcast_fusion), channel_id=1, source_target_pairs={{0,2},{1,3},{2,0},{3,1},{4,6},{5,7},{6,4},{7,5},{8,10},{9,11},{10,... | collective-permute-start | bytes 6291464 | tf_op jit(solution)/shard_map/ppermute | solution.py:431
  36.2 3.9 %copy-start.7 = (s32[8,5]{0,1:T(8,128)}, s32[8,5]{0,1:T(8,128)S(1)}, u32[]{:S(2)}) copy-start(s32[8,5]{0,1:T(8,128)S(1)} %reduce-window.9) | copy-start | bytes 484
  38.8 1.3 copy-start.2
  43.0 3.2 %copy-start.1 = (f32[256,4,2048]{0,2,1:T(8,128)}, f32[256,4,2048]{0,2,1:T(8,128)S(1)}, u32[]{:S(2)}) copy-start(f32[256,4,2048]{0,2,1:T(8,128)S(1)} %get-tuple-element.16) | copy-start | bytes 25165828
  43.0 3.2 %slice-start = ((s32[8,5]{0,1:T(8,128)}), s32[8,4]{0,1:T(4,128)S(1)}, s32[]{:S(2)}) async-start(s32[8,5]{0,1:T(8,128)} %copy-done.7), calls=%async_computation | async-start | bytes 4096 | tf_op jit(solution)/shard_map/slice.1
  46.5 5.9 %copy-start.9 = (f32[256,2]{0,1:T(2,128)S(1)}, f32[256,2]{0,1:T(2,128)}, u32[]{:S(2)}) copy-start(f32[256,2]{0,1:T(2,128)} %param.23) | copy-start | bytes 6148
  46.5 17.0 %copy-start.10 = (f32[256]{0:T(256)S(1)}, f32[256]{0:T(256)}, u32[]{:S(2)}) copy-start(f32[256]{0:T(256)} %param.24) | copy-start | bytes 3076
  65.0 76.2 %copy-start.3 = (bf16[256,512]{1,0:T(8,128)(2,1)S(1)}, bf16[256,512]{1,0:T(8,128)(2,1)}, u32[]{:S(2)}) copy-start(bf16[256,512]{1,0:T(8,128)(2,1)} %project_attended.1) | copy-start | bytes 786436
